TPU v7x, 1024 devices: a whole 4x4x32 slice. The times are simulated.
1024 devices in a mesh: kv: 128 (over z, y), tp: 8 (over x, core).
Axes of the slice: x: 4, y: 4, z: 32, core: 2. Of those that a mesh axis runs over, the one named last changes fastest.
Arguments:
- tokens: bfloat16 [16, 4096], P(None, 'kv')
- norm_gain: float32 [4096], P('kv'), may hold values from 0.1 to 1.9
- w_query: bfloat16 [4096, 3072], P('kv', 'tp'), may hold values from -0.09375 to 0.09375
- w_key: bfloat16 [4096, 3072], P('kv', 'tp'), may hold values from -0.09375 to 0.09375
- w_value: bfloat16 [4096, 3072], P('kv', 'tp'), may hold values from -0.09375 to 0.09375
- w_forget: bfloat16 [4096, 48], P('kv'), may hold values from -0.09375 to 0.09375
- w_out: bfloat16 [3072, 4096], P('tp', 'kv'), may hold values from -0.109375 to 0.109375
- mix_gain: float32 [4096], P('kv'), may hold values from 0.1 to 1.9
- w_up: bfloat16 [4096, 16384], P('kv', 'tp'), may hold values from -0.09375 to 0.09375
- w_down: bfloat16 [16384, 4096], P('tp', 'kv'), may hold values from -0.0625 to 0.0625
- key_cache: bfloat16 [16, 16384, 3072], P(None, 'kv', 'tp')
- value_cache: bfloat16 [16, 16384, 3072], P(None, 'kv', 'tp'), may hold values from -6 to 6
- decay_cache: float32 [16, 48, 16384], P(None, 'tp', 'kv')
- lengths: int32 [16], replicated, may hold values from 1 to 16384, 87381 in all
Outputs:
- layer_out: bfloat16 [16, 4096], P(None, 'kv')
Inputs may be any that keep to these rules, and one draw needn't show every extreme that they name: `lengths`: one sequence fills all 16384 positions.
All inputs are finite; a program needn't handle non-finite values.
Results may differ from a plain program's by a relative error of at most 0.01.
Values may be sent and summed in bfloat16 or wider, within the bound.
No kernel may reach another device: no remote copies, remote signals or barrier semaphores. Data moves between devices by JAX's collectives and lax.ppermute only.
A program may use at most 64 MiB of HBM per device.

v0:
```python
import jax
import jax.numpy as jnp
from jax import lax
from jax.sharding import Mesh
from jax.sharding import PartitionSpec as P

HEAD_DIM = 64
KV = ("kv_0", "kv_1")


epsilon = 1e-06
very_low = -1e30


def by_axis(x, axes):
    for axis in axes:
        x = lax.psum(x, axis)
    return x


def over_axes(x, axes):
    for axis in axes:
        x = lax.pmax(x, axis)
    return x


def copy_for_each(x, axis):
    size = lax.axis_size(axis)
    return lax.all_to_all(jnp.broadcast_to(x[None], (size, *x.shape)), axis, 0, 0, tiled=True)


def over_copies(x, axis):
    everything = copy_for_each(x, axis)
    return jnp.sum(everything, axis=0)


def summed_rows(x, axes, dim):
    if not axes:
        return x
    nearer = lax.psum_scatter(x, axes[0], scatter_dimension=dim, tiled=True)
    return summed_rows(nearer, axes[1:], dim)


def joined_along(tiles, dim):
    shape = list(tiles.shape[1:])
    shape[dim] *= tiles.shape[0]
    return jnp.moveaxis(tiles, 0, dim).reshape(shape)


def all_blocks(x, axes, turns):
    tiles = x
    for k in turns:
        tiles = lax.all_gather(tiles, axes[k])
    done = turns[::-1]
    back = [done.index(k) for k in range(len(axes))]
    tiles = tiles.transpose(*back, *range(len(axes), tiles.ndim))
    return tiles.reshape(-1, *x.shape)


def gathered_by_axis(x, axes, turns, dim):
    return joined_along(all_blocks(x, axes, turns), dim)


def local_softmax(query_heads, score_bias, keys_block, values_block, live_mask):
    rows_count, count = (keys_block.shape[0], keys_block.shape[1])
    heads_count = query_heads.shape[1]
    keys_view = keys_block.reshape(rows_count, count, heads_count, HEAD_DIM)
    values_view = values_block.reshape(rows_count, count, heads_count, HEAD_DIM)
    scores = jnp.einsum("bhe,bphe->bhp", query_heads, keys_view, preferred_element_type=jnp.float32)
    scores = scores * HEAD_DIM ** (-0.5) + score_bias
    block_peak = jnp.max(jnp.where(live_mask, scores, very_low), axis=2)
    weights = jnp.where(live_mask, jnp.exp(scores - block_peak[..., None]), 0.0)
    totals = jnp.sum(weights, axis=2)
    weighted = jnp.einsum(
        "bhp,bphe->bhe",
        weights.astype(jnp.bfloat16),
        values_view,
        preferred_element_type=jnp.float32,
    )
    return (block_peak, totals, weighted)


def shards(
    tokens,
    norm_gain,
    w_query,
    w_key,
    w_value,
    w_forget,
    w_out,
    mix_gain,
    w_up,
    w_down,
    key_cache,
    value_cache,
    decay_cache,
    lengths,
):
    rows_count = tokens.shape[0]
    width = tokens.shape[1] * lax.axis_size(KV)
    heads_here = decay_cache.shape[1]
    span = key_cache.shape[1]
    tokens_f = tokens.astype(jnp.float32)
    scaled_in = (tokens_f * norm_gain).astype(jnp.bfloat16)
    forget_cols = lax.dynamic_slice_in_dim(
        w_forget, lax.axis_index("tp") * heads_here, heads_here, 1
    )
    positions = lax.axis_index(KV) * span + jnp.arange(span, dtype=jnp.int32)
    newest = positions[None, None, :] == (lengths - 1)[:, None, None]
    summed = (
        by_axis(jnp.dot(scaled_in, w_query, preferred_element_type=jnp.float32), KV),
        by_axis(jnp.dot(scaled_in, w_key, preferred_element_type=jnp.float32), KV),
        by_axis(jnp.dot(scaled_in, w_value, preferred_element_type=jnp.float32), KV),
        by_axis(jnp.dot(scaled_in, forget_cols, preferred_element_type=jnp.float32), KV),
        by_axis(jnp.sum(tokens_f * tokens_f, axis=1), KV),
        by_axis(jnp.sum(jnp.where(newest, decay_cache, 0.0), axis=2), KV),
    )
    row_scale = lax.rsqrt(summed[4] / width + epsilon)[:, None]
    queries = (row_scale * summed[0]).astype(jnp.bfloat16)
    new_keys = (row_scale * summed[1]).astype(jnp.bfloat16)
    new_values = (row_scale * summed[2]).astype(jnp.bfloat16)
    now_decay = summed[5] + jax.nn.log_sigmoid(row_scale * summed[3])
    query_heads = queries.reshape(rows_count, heads_here, HEAD_DIM)
    own_score = jnp.sum(
        query_heads.astype(jnp.float32)
        * new_keys.astype(jnp.float32).reshape(rows_count, heads_here, HEAD_DIM),
        axis=2,
    ) * HEAD_DIM ** (-0.5)
    own_values = new_values.astype(jnp.float32).reshape(rows_count, heads_here, HEAD_DIM)
    live_mask = positions[None, None, :] < lengths[:, None, None]
    local_state = local_softmax(
        query_heads, now_decay[:, :, None] - decay_cache, key_cache, value_cache, live_mask
    )
    global_peak = over_axes(local_state[0], KV)
    highest = jnp.maximum(global_peak, own_score)
    factor_here = jnp.exp(local_state[0] - highest)
    total_sum, weighted_sum = (
        by_axis(local_state[1] * factor_here, KV),
        by_axis(local_state[2] * factor_here[..., None], KV),
    )
    factor_own = jnp.exp(own_score - highest)
    final_state = (
        highest,
        total_sum + factor_own,
        weighted_sum + factor_own[..., None] * own_values,
    )
    attended = (
        (final_state[2] / final_state[1][..., None])
        .reshape(rows_count, heads_here * HEAD_DIM)
        .astype(jnp.bfloat16)
    )
    head_terms = over_copies(jnp.dot(attended, w_out, preferred_element_type=jnp.float32), "tp")
    mixed_f = (tokens_f + head_terms).astype(jnp.bfloat16).astype(jnp.float32)
    mix_in = (mixed_f * mix_gain).astype(jnp.bfloat16)
    up_terms = jnp.dot(mix_in, w_up, preferred_element_type=jnp.float32)
    squares_here = jnp.sum(mixed_f * mixed_f, axis=1)
    up_share = summed_rows(up_terms, KV, 1)
    squares_all = by_axis(squares_here, KV)
    mix_scale = lax.rsqrt(squares_all / width + epsilon)[:, None]
    hidden_share = (jax.nn.relu(mix_scale * up_share) ** 2).astype(jnp.bfloat16)
    down_terms = jnp.dot(
        gathered_by_axis(hidden_share, KV, (0, 1), 1), w_down, preferred_element_type=jnp.float32
    )
    channel_terms = over_copies(down_terms, "tp")
    return (mixed_f + channel_terms).astype(jnp.bfloat16)


def solution(mesh):
    torus = Mesh(mesh.devices.reshape(32, 4, mesh.shape["tp"]), ("kv_0", "kv_1", "tp"))
    placed = (
        P(None, KV),
        P(KV),
        P(KV, "tp"),
        P(KV, "tp"),
        P(KV, "tp"),
        P(KV, None),
        P("tp", KV),
        P(KV),
        P(KV, "tp"),
        P("tp", KV),
        P(None, KV, "tp"),
        P(None, KV, "tp"),
        P(None, "tp", KV),
        P(),
    )
    return jax.shard_map(
        shards, mesh=torus, in_specs=placed, out_specs=P(None, KV), check_vma=False
    )
```

profile of v0, /device:TPU:1, one launch (start us, length us, event | category | flops | bytes accessed | tf_op | source)
XLA Modules:
  0.0 608.3 jit_solution(12604490867263633869)
XLA Ops:
  6.5 0.7 broadcast_add_fusion
  7.2 0.8 fusion.8
  8.0 0.9 fusion.22
  8.9 0.9 fusion.25
  9.8 1.0 fusion.14
  10.8 0.7 broadcast_compare_fusion
  11.5 0.9 select_reduce_fusion.1
  12.4 94.5 %all-reduce.1 = (f32[16,384]{1,0:T(8,128)S(1)}, f32[16]{0:T(128)S(1)}, f32[16,6]{0,1:T(8,128)S(1)}, f32[16,6]{0,1:T(8,128)S(1)}, f32[16,384]{1,0:T(8,128)S(1)}) all-reduce(f32[16,384]{1,0:T(8,128)S(1)} %fusion.25, f32[16]{0:T(128)S(1)} %fusion.8, ...), channel_id=1, replica_groups=mesh['kv_0'=32,'kv_1'=4,'tp'=8] {'kv_0'}, use_global_device_ids=true, to_apply=%region_3.0 | all-reduce | flops 12496 | bytes 99968 | tf_op jit(solution)/shard_map/psum | solution.py:17
  106.9 14.1 %all-reduce.3 = (f32[16,384]{1,0:T(8,128)S(1)}, f32[16]{0:T(128)S(1)}, f32[16,6]{0,1:T(8,128)S(1)}, f32[16,6]{0,1:T(8,128)S(1)}, f32[16,384]{1,0:T(8,128)S(1)}) all-reduce(f32[16,384]{1,0:T(8,128)S(1)} %get-tuple-element.8, f32[16]{0:T(128)S(1)} %get-tuple-element.9, ...), channel_id=1, replica_groups=mesh['kv_0'=32,'kv_1'=4,'tp'=8] {'kv_1'}, use_global_device_ids=true, to_apply=%region_4.0 | all-reduce | flops 12496 | bytes 99968 | tf_op jit(solution)/shard_map/psum | solution.py:17
  121.6 1.9 copy.45
  124.4 39.1 %pmax.14 = f32[16,6]{0,1:T(8,128)S(1)} all-reduce(f32[16,6]{0,1:T(8,128)S(1)} %get-tuple-element.27), channel_id=1, replica_groups=mesh['kv_0'=32,'kv_1'=4,'tp'=8] {'kv_0'}, use_global_device_ids=true, to_apply=%region_11.12 | all-reduce | flops 96 | bytes 768 | tf_op jit(solution)/shard_map/pmax | solution.py:23
  163.7 6.0 pmax.15
  169.8 1.0 copy.46
  170.9 0.9 fusion.1
  172.0 78.1 %all-reduce = (f32[16,6,64]{2,1,0:T(8,128)S(1)}, f32[16,384]{1,0:T(8,128)S(1)}, f32[16,6]{0,1:T(8,128)S(1)}) all-reduce(f32[16,6,64]{2,1,0:T(8,128)S(1)} %bitcast_multiply_fusion, f32[16,384]{1,0:T(8,128)S(1)} %fusion.20, f32[16,6]{0,1:T(8,128)S(1)} %get-tuple-element.25), channel_id=1, replica_groups=mesh['kv_0'=32,'kv_1'=4,'tp'=8] {'kv_0'}, use_global_device_ids=true, to_apply=%region_16.17 | all-reduce | flops 12384 | bytes 99072 | tf_op jit(solution)/shard_map/psum | solution.py:17
  250.1 14.0 %all-reduce.2 = (f32[16,6,64]{2,1,0:T(8,128)S(1)}, f32[16,384]{1,0:T(8,128)S(1)}, f32[16,6]{0,1:T(8,128)S(1)}) all-reduce(f32[16,6,64]{2,1,0:T(8,128)S(1)} %get-tuple-element.5, f32[16,384]{1,0:T(8,128)S(1)} %get-tuple-element.6, f32[16,6]{0,1:T(8,128)S(1)} %get-tuple-element.7), channel_id=1, replica_groups=mesh['kv_0'=32,'kv_1'=4,'tp'=8] {'kv_1'}, use_global_device_ids=true, to_apply=%region_17.18 | all-reduce | flops 12384 | bytes 99072 | tf_op jit(solution)/shard_map/psum | solution.py:17
  264.8 86.8 %all_to_all.10 = f32[8,1,512]{2,1,0:T(1,128)S(1)} all-to-all(f32[8,1,512]{2,1,0:T(1,128)S(1)} %reshape.127), channel_id=1, replica_groups=mesh['kv_0'=32,'kv_1'=4,'tp'=8] {'tp'}, dimensions={0} | all-to-all | bytes 32768 | tf_op jit(solution)/shard_map/all_to_all | solution.py:29
  352.2 0.7 reduce
  353.1 1.3 convolution_bitcast_fusion
  354.5 39.6 %psum.142 = f32[16]{0:T(128)S(1)} all-reduce(f32[16]{0:T(128)S(1)} %get-tuple-element.21), channel_id=1, replica_groups=mesh['kv_0'=32,'kv_1'=4,'tp'=8] {'kv_0'}, use_global_device_ids=true, to_apply=%region_25.26 | all-reduce | flops 16 | bytes 128 | tf_op jit(solution)/shard_map/psum | solution.py:17
  394.2 6.4 %psum.143 = f32[16]{0:T(128)S(1)} all-reduce(f32[16]{0:T(128)S(1)} %psum.142), channel_id=1, replica_groups=mesh['kv_0'=32,'kv_1'=4,'tp'=8] {'kv_1'}, use_global_device_ids=true, to_apply=%region_26.27 | all-reduce | flops 16 | bytes 128 | tf_op jit(solution)/shard_map/psum | solution.py:17
  400.5 55.2 %reduce-scatter.7.cloned.1.call-done = f32[64,16]{1,0:T(8,128)} async-done(((f32[2048,16]{1,0:T(8,128)}), f32[64,16]{1,0:T(8,128)}) %reduce-scatter.7.cloned.1.call-update) | async-done | bytes 4112
  455.8 58.4 %reduce-scatter.9.cloned.1.call-done = f32[16,16]{1,0:T(8,128)} async-done(((f32[64,16]{1,0:T(8,128)}), f32[16,16]{1,0:T(8,128)}) %reduce-scatter.9.cloned.1.call-update) | async-done | bytes 1040
  514.2 0.8 copy.62
  515.1 44.6 %all-gather = bf16[512,16]{1,0:T(8,128)(2,1)S(1)} all-gather(bf16[16,16]{1,0:T(8,128)(2,1)S(1)} %multiply_convert_fusion.3), channel_id=2, replica_groups=mesh['kv_0'=32,'kv_1'=4,'tp'=8] {'kv_0'}, dimensions={0}, use_global_device_ids=true | all-gather | bytes 16896 | tf_op jit(solution)/shard_map/all_gather | solution.py:53
  559.7 9.9 %all-gather.1 = bf16[128,16,16]{2,1,0:T(8,128)(2,1)S(1)} all-gather(bf16[32,16,16]{2,1,0:T(8,128)(2,1)S(1)} %bitcast.39), channel_id=3, replica_groups=mesh['kv_0'=32,'kv_1'=4,'tp'=8] {'kv_1'}, dimensions={0}, use_global_device_ids=true | all-gather | bytes 81920 | tf_op jit(solution)/shard_map/all_gather | solution.py:53
  569.6 0.5 copy.58
  570.1 0.9 copy.52
  571.2 0.8 reshape.108
  572.3 27.8 %all_to_all.11 = f32[8,1,512]{2,1,0:T(1,128)S(1)} all-to-all(f32[8,1,512]{2,1,0:T(1,128)S(1)} %reshape.129), channel_id=1, replica_groups=mesh['kv_0'=32,'kv_1'=4,'tp'=8] {'tp'}, dimensions={0} | all-to-all | bytes 32768 | tf_op jit(solution)/shard_map/all_to_all | solution.py:29
  600.1 0.7 reduce.1
  600.9 0.6 fusion.13
  (60 shorter events, 4.1 us)
Async XLA Ops:
  6.5 346.6 %copy-start = (bf16[32,2048]{1,0:T(8,128)(2,1)S(1)}, bf16[32,2048]{1,0:T(8,128)(2,1)}, u32[]{:S(2)}) copy-start(bf16[32,2048]{1,0:T(8,128)(2,1)} %param.22) | copy-start | bytes 393220
  6.5 449.2 %reduce-scatter.7.cloned.1.call-start = ((), (), s32[]{:S(2)}) async-start(), calls=%async_computation.4 | async-start | bytes 1081344
  123.5 0.8 copy-start.2
  123.5 46.3 %copy-start.1 = (bf16[16,128,384]{2,1,0:T(8,128)(2,1)S(1)}, bf16[16,128,384]{2,1,0:T(8,128)(2,1)}, u32[]{:S(2)}) copy-start(bf16[16,128,384]{2,1,0:T(8,128)(2,1)} %param.25) | copy-start | bytes 4718596
  169.8 1.0 copy-start.3
  169.8 1.0 copy-start.5
  169.8 1.0 copy-start.7
  170.8 93.8 %copy-start.6 = (bf16[384,32]{0,1:T(8,128)(2,1)S(1)}, bf16[384,32]{0,1:T(8,128)(2,1)}, u32[]{:S(2)}) copy-start(bf16[384,32]{0,1:T(8,128)(2,1)} %param.20) | copy-start | bytes 73732
  170.8 182.3 %copy-start.8 = (f32[32]{0:T(128)S(1)}, f32[32]{0:T(128)}, u32[]{:S(2)}) copy-start(f32[32]{0:T(128)} %param.21) | copy-start | bytes 388
  354.5 159.8 %reduce-scatter.9.cloned.1.call-start = ((), (), s32[]{:S(2)}) async-start(), calls=%async_computation.5 | async-start | bytes 40960
  569.6 2.4 copy-start.4
Sparse Core Ops, SparseCore 0:
  354.6 101.1 reduce-scatter.6
  459.1 55.0 reduce-scatter.8
where the time goes:
time: 609 us; the launch traced here: 608 us
  blocking collectives  461 us (76%)
  waiting for transfers between devices  114 us (19%)
  between operations  13.7 us (2%)
  local copies, waits for them, and re-layouts  7.96 us (1%)
  other arithmetic  6.11 us (1%)
    psum x6, blocking collectives, by_axis(): x = lax.psum(x, axis)  247 us
    all_to_all x2, blocking collectives, copy_for_each(): lax.all_to_all(jnp.broadcast_to(x[None], (size, *x.shape)), axis, 0, 0, t...  115 us
    unnamed x4, waiting for transfers between devices  114 us
    all_gather x2, blocking collectives, all_blocks(): tiles = lax.all_gather(tiles, axes[k])  54.5 us
    pmax x2, blocking collectives, over_axes(): x = lax.pmax(x, axis)  45.1 us
  transfers between devices with their start and end apart: 2, of which 2 were waited for; matrix products, arithmetic and copies ran while one was open for 0% of the time, Pallas kernels for 0%

commit v1 on v0

v1 whole, which is shorter than its diff:
```python
import jax
import jax.numpy as jnp
from jax import lax
from jax.experimental import pallas as pl
from jax.experimental.pallas import tpu as pltpu
from jax.sharding import Mesh
from jax.sharding import PartitionSpec as P

HEAD_DIM = 64
LANES = 128
KV = ("kv_0", "kv_1")
epsilon = 1e-06
very_low = -1e30
f32 = jnp.float32
bf16 = jnp.bfloat16

VMEM = pl.BlockSpec(memory_space=pltpu.VMEM)
SMEM = pl.BlockSpec(memory_space=pltpu.SMEM)
NT = (((1,), (1,)), ((), ()))


def exchanged(x, axes):
    return lax.all_to_all(x, axes, 0, 0, tiled=True)


def lane_of(shape):
    return lax.broadcasted_iota(jnp.int32, shape, len(shape) - 1)


def split_in_three(x):
    high = lax.reduce_precision(x, 8, 7)
    rest = x - high
    middle = lax.reduce_precision(rest, 8, 7)
    return high, middle, rest - middle


def length_column(lengths_ref, rows, width):
    row = lax.broadcasted_iota(jnp.int32, (rows, width), 0)
    out = jnp.zeros((rows, width), jnp.int32)
    for b in range(rows):
        out = jnp.where(row == b, lengths_ref[b], out)
    return out


def first_position(span):
    return (lax.axis_index("kv_0") * lax.axis_size("kv_1") + lax.axis_index("kv_1")) * span


def project_kernel(tokens, gain, w_query, w_key, w_value, w_forget, decay, lengths, out):
    rows = tokens.shape[0]
    heads = decay.shape[0]
    span = decay.shape[2]
    slots = out.shape[0] // rows
    x = tokens[...].astype(f32)
    scaled = (x * gain[...]).astype(bf16)
    q = jnp.dot(scaled, w_query[...], preferred_element_type=f32)
    k = jnp.dot(scaled, w_key[...], preferred_element_type=f32)
    v = jnp.dot(scaled, w_value[...], preferred_element_type=f32)
    gates = jnp.dot(scaled, w_forget[...], preferred_element_type=f32)
    squares = jnp.sum(x * x, axis=1, keepdims=True)
    position = first_position(span) + lane_of((rows, span))
    newest = position == length_column(lengths, rows, span) - 1
    gate_lane = lane_of(gates.shape)
    lane = lane_of((rows, HEAD_DIM))
    first_head = lax.axis_index("tp") * heads
    for h in range(slots):
        if h < heads:
            cols = slice(h * HEAD_DIM, (h + 1) * HEAD_DIM)
            gate = jnp.sum(jnp.where(gate_lane == first_head + h, gates, 0.0), axis=1, keepdims=True)
            last = jnp.sum(jnp.where(newest, decay[h], 0.0), axis=1, keepdims=True)
            high, middle, low = split_in_three(last)
            extra = jnp.where(lane == 0, gate, 0.0)
            extra = jnp.where(lane == 1, high, extra)
            extra = jnp.where(lane == 2, middle, extra)
            extra = jnp.where(lane == 3, low, extra)
            extra = jnp.where(lane == 4, squares, extra)
            top = jnp.concatenate([q[:, cols], k[:, cols]], axis=1)
            bottom = jnp.concatenate([v[:, cols], extra], axis=1)
        else:
            top = bottom = jnp.zeros((rows, LANES), f32)
        for b in range(rows):
            both = jnp.concatenate([top[b : b + 1], bottom[b : b + 1]], axis=0)
            out[b * slots + h] = both.astype(bf16)


def query_kernel(width, got, out, state):
    total = jnp.sum(got[...].astype(f32), axis=0)
    top, bottom = total[0:1], total[1:2]
    lane = lane_of((1, LANES))
    pick = lambda i: jnp.sum(jnp.where(lane == HEAD_DIM + i, bottom, 0.0), axis=1, keepdims=True)
    row_scale = lax.rsqrt(pick(4) / width + epsilon)
    top = (row_scale * top).astype(bf16).astype(f32)
    value = (row_scale * bottom).astype(bf16).astype(f32)
    own = (
        jnp.sum(top[:, :HEAD_DIM] * top[:, HEAD_DIM:], axis=1, keepdims=True) * HEAD_DIM ** (-0.5)
    )
    gate = row_scale * pick(0)
    log_forget = jnp.minimum(gate, 0.0) - jnp.log1p(jnp.exp(-jnp.abs(gate)))
    now_decay = pick(1) + pick(2) + pick(3) + log_forget
    out[...] = jnp.broadcast_to(top[None], out.shape)
    row = jnp.where(lane == HEAD_DIM, own, value)
    row = jnp.where(lane == HEAD_DIM + 1, now_decay, row)
    state[...] = jnp.broadcast_to(row, state.shape)


def attend_kernel(queries, keys, values, decay, lengths, out):
    rows, slots, _ = queries.shape
    heads = decay.shape[0]
    span = keys.shape[1]
    channels = keys.shape[2]
    position = first_position(span) + lane_of((slots, span))
    mine = lane_of((slots, channels)) // HEAD_DIM == lax.broadcasted_iota(
        jnp.int32, (slots, channels), 0
    )
    lane = lane_of((slots, HEAD_DIM))
    for b in range(rows):
        q = queries[b][:, :HEAD_DIM] * HEAD_DIM ** (-0.5)
        q = jnp.concatenate([q] * heads, axis=1)
        q = jnp.where(mine, q, 0.0).astype(bf16)
        scores = lax.dot_general(q, keys[b], NT, preferred_element_type=f32)
        parts = [decay[h, b : b + 1, :] for h in range(heads)]
        if slots > heads:
            parts.append(jnp.zeros((slots - heads, span), f32))
        scores = scores - jnp.concatenate(parts, axis=0)
        live = position < lengths[b]
        peak = jnp.max(jnp.where(live, scores, very_low), axis=1, keepdims=True)
        weights = jnp.where(live, jnp.exp(scores - peak), 0.0)
        total = jnp.sum(weights, axis=1, keepdims=True)
        mixed = jnp.dot(weights.astype(bf16), values[b], preferred_element_type=f32)
        mixed = jnp.where(mine, mixed, 0.0)
        folded = mixed[:, :HEAD_DIM]
        for h in range(1, heads):
            folded = folded + mixed[:, h * HEAD_DIM : (h + 1) * HEAD_DIM]
        tail = jnp.where(lane == 0, peak, jnp.where(lane == 1, total, 0.0))
        out[b] = jnp.concatenate([folded, tail], axis=1)


def combine_kernel(got, state, out):
    rows, slots, _ = got.shape
    r = got[...].reshape(rows * slots, LANES)
    row = state[0:1]
    lane = lane_of((1, LANES))
    own = jnp.sum(jnp.where(lane == HEAD_DIM, row, 0.0), axis=1, keepdims=True)
    now_decay = jnp.sum(jnp.where(lane == HEAD_DIM + 1, row, 0.0), axis=1, keepdims=True)
    peaks = r[:, HEAD_DIM : HEAD_DIM + 1] + now_decay
    peak = jnp.maximum(jnp.max(peaks, axis=0, keepdims=True), own)
    acc = jnp.sum(jnp.exp(peaks - peak) * r, axis=0, keepdims=True)
    mine = jnp.exp(own - peak)
    total = jnp.sum(jnp.where(lane == HEAD_DIM + 1, acc, 0.0), axis=1, keepdims=True) + mine
    attended = (acc + mine * row) / total
    attended = attended.astype(bf16).astype(f32)
    out[...] = jnp.broadcast_to(attended[None], out.shape)


def output_kernel(heads, got, block, out, aside):
    attended = jnp.concatenate([got[:, h, :][:, :HEAD_DIM] for h in range(heads)], axis=1)
    channels = heads * HEAD_DIM
    terms = lax.dot_general(
        attended.astype(bf16), block[:, :channels], NT, preferred_element_type=f32
    ).astype(bf16)
    for i in range(out.shape[0]):
        out[i] = terms
    turned = block[:, channels:].astype(f32).T
    aside[...] = turned[: aside.shape[0]]


def up_kernel(got, aside, w_up, out, mixed_out):
    rows = got.shape[1]
    terms = got[0].astype(f32)
    for i in range(1, got.shape[0]):
        terms = terms + got[i].astype(f32)
    gain = aside[rows : rows + 1] + aside[rows + 1 : rows + 2] + aside[rows + 2 : rows + 3]
    mixed = (aside[:rows] + terms).astype(bf16)
    mixed_out[...] = mixed
    mixed = mixed.astype(f32)
    squares = jnp.sum(mixed * mixed, axis=1, keepdims=True)
    high, middle, low = split_in_three(squares)
    up = jnp.dot((mixed * gain).astype(bf16), w_up[...], preferred_element_type=f32).astype(bf16)
    lane = lane_of((rows, LANES))
    tail = jnp.where(lane == 0, high, jnp.where(lane == 1, middle, jnp.where(lane == 2, low, 0.0)))
    tail = tail.astype(bf16)
    hidden = up.shape[1]
    for i in range(out.shape[0]):
        out[i, :, :hidden] = up
        out[i, :, hidden:] = tail


def down_kernel(width, got, w_down, out):
    hidden = w_down.shape[1]
    total = got[0].astype(f32)
    for i in range(1, got.shape[0]):
        total = total + got[i].astype(f32)
    squares = jnp.sum(total[:, hidden:], axis=1, keepdims=True)
    mix_scale = lax.rsqrt(squares / width + epsilon)
    live = jnp.maximum(mix_scale * total[:, :hidden], 0.0)
    terms = lax.dot_general(
        (live * live).astype(bf16), w_down[...], NT, preferred_element_type=f32
    )
    rows, columns = terms.shape
    terms = jnp.concatenate([terms, jnp.zeros((rows, LANES - columns), f32)], axis=1)
    for i in range(out.shape[0]):
        out[i] = terms


def room(mebibytes):
    return pltpu.CompilerParams(vmem_limit_bytes=mebibytes << 20)


def call(kernel, outs, *args, specs=None, mebibytes=8):
    return pl.pallas_call(
        kernel,
        out_shape=outs,
        compiler_params=room(mebibytes),
        in_specs=specs or [VMEM] * len(args),
        out_specs=jax.tree.map(lambda _: VMEM, outs),
    )(*args)


def shaped(shape, dtype):
    return jax.ShapeDtypeStruct(shape, dtype)


def shards(
    tokens,
    norm_gain,
    w_query,
    w_key,
    w_value,
    w_forget,
    w_out,
    mix_gain,
    w_up,
    w_down,
    key_cache,
    value_cache,
    decay_cache,
    lengths,
):
    rows, features = tokens.shape
    devices = lax.axis_size(KV)
    far = lax.axis_size("kv_0")
    near = lax.axis_size("kv_1")
    groups = lax.axis_size("tp")
    width = features * devices
    heads = decay_cache.shape[1]
    slots = devices // rows
    hidden = w_up.shape[1]
    decay = jnp.transpose(decay_cache, (1, 0, 2))
    gain_parts = jnp.stack(split_in_three(mix_gain)).astype(bf16)
    aside = jnp.concatenate([tokens, gain_parts], axis=0).T
    aside = jnp.pad(aside, ((0, 0), (0, LANES - aside.shape[1])))
    bundle = jnp.concatenate([w_up, w_out.T, aside], axis=1)
    gathered = lax.all_gather(bundle, "kv_0", tiled=True)
    side = bundle.shape[1] - hidden
    deep = gathered.shape[0]

    pieces = call(
        project_kernel,
        shaped((devices, 2, LANES), bf16),
        tokens,
        norm_gain[None],
        w_query,
        w_key,
        w_value,
        w_forget,
        decay,
        lengths,
        specs=[VMEM] * 7 + [SMEM],
    )
    got = exchanged(pieces, KV)
    spread, state = call(
        lambda *refs: query_kernel(width, *refs),
        (shaped((rows, slots, LANES), f32), shaped((8, LANES), f32)),
        got,
    )
    got = exchanged(spread.reshape(devices, 1, LANES), KV).reshape(rows, slots, LANES)
    local = call(
        attend_kernel,
        shaped((rows, slots, LANES), f32),
        got,
        key_cache,
        value_cache,
        decay,
        lengths,
        specs=[VMEM] * 4 + [SMEM],
    )
    got = exchanged(local.reshape(devices, 1, LANES), KV).reshape(rows, slots, LANES)
    spread = call(combine_kernel, shaped((rows, slots, LANES), f32), got, state)
    got = exchanged(spread.reshape(devices, 1, LANES), KV).reshape(rows, slots, LANES)
    whole = lambda shape: pl.BlockSpec(shape, lambda i: (0,) * len(shape))
    terms, aside = pl.pallas_call(
        lambda *refs: output_kernel(heads, *refs),
        grid=(1,),
        compiler_params=room(8),
        out_shape=(shaped((groups, rows, deep), bf16), shaped((rows + 8, deep), f32)),
        in_specs=[whole(got.shape), pl.BlockSpec((deep, side), lambda i: (0, hidden // side))],
        out_specs=(whole((groups, rows, deep)), whole((rows + 8, deep))),
    )(got, gathered)
    got = exchanged(terms, "tp")
    up, mixed = pl.pallas_call(
        up_kernel,
        grid=(1,),
        compiler_params=room(16),
        out_shape=(shaped((near, rows, hidden + LANES), bf16), shaped((rows, deep), bf16)),
        in_specs=[
            whole(got.shape),
            whole(aside.shape),
            pl.BlockSpec((deep, hidden), lambda i: (0, 0)),
        ],
        out_specs=(whole((near, rows, hidden + LANES)), whole((rows, deep))),
    )(got, aside, gathered)
    got = exchanged(up, "kv_1")
    down = call(
        lambda *refs: down_kernel(width, *refs),
        shaped((groups, rows, LANES), f32),
        got,
        w_down.T,
    )
    got = exchanged(down, "tp")
    mine = lax.dynamic_slice_in_dim(mixed, lax.axis_index("kv_0") * features, features, 1)
    total = jnp.sum(got, axis=0)[:, :features]
    return (mine.astype(f32) + total).astype(bf16)


def solution(mesh):
    near = 4
    far = mesh.shape["kv"] // near
    torus = Mesh(
        mesh.devices.reshape(far, near, mesh.shape["tp"]), ("kv_0", "kv_1", "tp")
    )
    placed = (
        P(None, KV),
        P(KV),
        P(KV, "tp"),
        P(KV, "tp"),
        P(KV, "tp"),
        P(KV, None),
        P("tp", KV),
        P(KV),
        P(KV, "tp"),
        P("tp", KV),
        P(None, KV, "tp"),
        P(None, KV, "tp"),
        P(None, "tp", KV),
        P(),
    )
    return jax.shard_map(
        shards, mesh=torus, in_specs=placed, out_specs=P(None, KV), check_vma=False
    )
```

time: 609 us -> 226 us (0.37)
  blocking collectives: 461 us -> 175 us
  waiting for transfers between devices: 114 us -> 4.89 us
  Pallas kernels: 0 us -> 8.81 us
    psum x6 -> x0, blocking collectives: 247 us -> none  [by_axis(): x = lax.psum(x, axis)]
    unnamed x4 -> x1, waiting for transfers between devices: 114 us -> 0.02 us
    all_to_all x2 -> x6, blocking collectives: 115 us -> 175 us  [exchanged(): return lax.all_to_all(x, axes, 0, 0, tiled=True)]
    all_gather x2 -> x0, blocking collectives: 54.5 us -> none  [all_blocks(): tiles = lax.all_gather(tiles, axes[k])]
    pmax x2 -> x0, blocking collectives: 45.1 us -> none  [over_axes(): x = lax.pmax(x, axis)]
    unnamed x25 -> x31, local copies, waits for them, and re-layouts: 4.28 us -> 13.3 us
    pallas_call x0 -> x7, Pallas kernels: none -> 8.81 us  [the longest x5 7.81 us: call(): pl.pallas_call(kernel, out_shape=outs, compiler_params=room(mebibytes), i...]
  transfers between devices with their start and end apart: 2 -> 2, of which waited for: 2 -> 1; matrix products, arithmetic and copies ran while one was open for 0% -> 0% of each run, Pallas kernels for 0% -> 3%
where the time goes in v1:
time: 226 us; the launch traced here: 225 us
  blocking collectives  175 us (77%)
  local copies, waits for them, and re-layouts  13.6 us (6%)
  between operations  13.4 us (6%)
  Pallas kernels  8.81 us (4%)
  starting transfers between devices  5.72 us (3%)
  waiting for transfers between devices  4.89 us (2%)
  other arithmetic  3.04 us (1%)
    all_to_all x6, blocking collectives, exchanged(): return lax.all_to_all(x, axes, 0, 0, tiled=True)  175 us
    unnamed x31, local copies, waits for them, and re-layouts  13.3 us
    pallas_call x5, Pallas kernels, call(): pl.pallas_call(kernel, out_shape=outs, compiler_params=room(mebibytes), i...  7.81 us
    all_to_all x1, starting transfers between devices, exchanged(): return lax.all_to_all(x, axes, 0, 0, tiled=True)  5.72 us
    all_to_all x1, waiting for transfers between devices, exchanged(): return lax.all_to_all(x, axes, 0, 0, tiled=True)  4.87 us
  transfers between devices with their start and end apart: 2, of which 1 were waited for; matrix products, arithmetic and copies ran while one was open for 0% of the time, Pallas kernels for 3%

profile of v1, /device:TPU:1, one launch (start us, length us, event | category | flops | bytes accessed | tf_op | source)
XLA Modules:
  0.0 224.7 jit_solution(17710241600341729675)
XLA Ops:
  6.5 0.7 fusion.3
  7.5 0.8 copy.22
  8.4 1.6 fusion.1
  10.0 0.8 copy-done.4
  10.8 0.7 copy-done.7
  11.5 0.7 copy-done.8
  12.3 0.7 copy-done.9
  13.0 0.7 copy-done.10
  13.7 0.7 copy-done.11
  14.4 0.7 copy-done.12
  15.0 0.7 copy-done.14
  15.7 0.9 shard_map.136
  16.6 57.7 %all_to_all.35.refs_0_ = bf16[128,2,128]{2,1,0:T(2,128)(2,1)S(1)} all-to-all(bf16[128,2,128]{2,1,0:T(2,128)(2,1)S(1)} %shard_map.136), channel_id=1, replica_groups=mesh['kv_0'=32,'kv_1'=4,'tp'=8] {'kv_0','kv_1'}, dimensions={0} | all-to-all | bytes 131072 | tf_op jit(solution)/shard_map/all_to_all | solution.py:23
  74.3 0.4 shard_map.137
  74.7 31.8 %all_to_all.36 = f32[128,1,128]{2,1,0:T(1,128)S(1)} all-to-all(f32[128,1,128]{2,1,0:T(1,128)S(1)} %bitcast.32), channel_id=1, replica_groups=mesh['kv_0'=32,'kv_1'=4,'tp'=8] {'kv_0','kv_1'}, dimensions={0} | all-to-all | bytes 131072 | tf_op jit(solution)/shard_map/all_to_all | solution.py:23
  106.4 1.4 copy-done.2
  107.9 1.4 copy-done.3
  109.3 0.8 copy-done.5
  110.1 0.7 copy-done.13
  110.7 5.3 %shard_map.138 = f32[16,8,128]{2,1,0:T(8,128)S(1)} custom-call(f32[16,8,128]{2,1,0:T(8,128)S(1)} %bitcast.24, bf16[16,128,384]{2,1,0:T(8,128)(2,1)S(1)} %copy-done.2, bf16[16,128,384]{2,1,0:T(8,128)(2,1)S(1)} %copy-done.3, f32[6,16,128]{2,1,0:T(8,128)S(1)} %bitcast.30, s32[16]{0:T(128)S(1)} %copy-done.13), custom_call_target="tpu_custom_call" | custom-call | tf_op jit(solution)/shard_map/pallas_call | solution.py:210
  116.0 31.9 %all_to_all.37 = f32[128,1,128]{2,1,0:T(1,128)S(1)} all-to-all(f32[128,1,128]{2,1,0:T(1,128)S(1)} %bitcast.25), channel_id=1, replica_groups=mesh['kv_0'=32,'kv_1'=4,'tp'=8] {'kv_0','kv_1'}, dimensions={0} | all-to-all | bytes 131072 | tf_op jit(solution)/shard_map/all_to_all | solution.py:23
  148.0 0.4 shard_map.139
  148.3 30.3 %all_to_all.38 = f32[128,1,128]{2,1,0:T(1,128)S(1)} all-to-all(f32[128,1,128]{2,1,0:T(1,128)S(1)} %bitcast.27), channel_id=1, replica_groups=mesh['kv_0'=32,'kv_1'=4,'tp'=8] {'kv_0','kv_1'}, dimensions={0} | all-to-all | bytes 131072 | tf_op jit(solution)/shard_map/all_to_all | solution.py:23
  178.7 2.5 %copy-done = bf16[1024,2560]{1,0:T(8,128)(2,1)S(1)} copy-done((bf16[1024,2560]{1,0:T(8,128)(2,1)S(1)}, bf16[1024,2560]{1,0:T(8,128)(2,1)}, u32[]{:S(2)}) %copy-start) | copy-done | bytes 5242904
  181.2 0.3 shard_map.140
  181.5 15.4 %all_to_all.39.got = bf16[8,16,1024]{2,1,0:T(8,128)(2,1)S(1)} all-to-all(bf16[8,16,1024]{2,1,0:T(8,128)(2,1)S(1)} %get-tuple-element.13), channel_id=1, replica_groups=mesh['kv_0'=32,'kv_1'=4,'tp'=8] {'tp'}, dimensions={0} | all-to-all | bytes 524288 | tf_op jit(solution)/shard_map/all_to_all | solution.py:23
  196.9 0.7 shard_map.141
  197.6 8.1 %all_to_all.40.refs_0_ = bf16[4,16,2176]{2,1,0:T(8,128)(2,1)S(1)} all-to-all(bf16[4,16,2176]{2,1,0:T(8,128)(2,1)S(1)} %get-tuple-element.16), channel_id=1, replica_groups=mesh['kv_0'=32,'kv_1'=4,'tp'=8] {'kv_1'}, dimensions={0} | all-to-all | bytes 557056 | tf_op jit(solution)/shard_map/all_to_all | solution.py:23
  205.7 0.9 shard_map.142
  206.6 5.7 %all-to-all-start.6 = ((f32[8,16,128]{2,1,0:T(8,128)}), f32[8,16,128]{2,1,0:T(8,128)S(1)}, u32[]{:S(2)}, u32[]{:S(2)}) async-start(f32[8,16,128]{2,1,0:T(8,128)} %shard_map.142), calls=%async_computation.6 | async-start | bytes 131072 | tf_op jit(solution)/shard_map/all_to_all | solution.py:23
  212.3 4.9 %all-to-all-done.6 = f32[8,16,128]{2,1,0:T(8,128)S(1)} async-done(((f32[8,16,128]{2,1,0:T(8,128)}), f32[8,16,128]{2,1,0:T(8,128)S(1)}, u32[]{:S(2)}, u32[]{:S(2)}) %all-to-all-start.6) | async-done | bytes 65568 | tf_op jit(solution)/shard_map/all_to_all | solution.py:23
  217.2 0.7 fusion.2
  (25 shorter events, 0.4 us)
Async XLA Ops:
  6.5 172.1 %all-gather.2.cloned.1.call-start = ((), (), s32[]{:S(2)}) async-start(), calls=%async_computation.7 | async-start | bytes 5406720 | tf_op jit(solution)/shard_map/all_gather | solution.py:253
  10.0 0.8 copy-start.4
  10.8 0.7 copy-start.7
  11.5 0.7 copy-start.8
  12.3 0.7 copy-start.9
  13.0 0.7 copy-start.10
  13.7 0.7 copy-start.11
  14.4 0.7 copy-start.12
  15.0 0.7 copy-start.14
  106.4 1.4 copy-start.2
  107.9 1.4 copy-start.3
  109.3 0.8 copy-start.5
  110.1 0.7 copy-start.13
  178.7 2.5 %copy-start = (bf16[1024,2560]{1,0:T(8,128)(2,1)S(1)}, bf16[1024,2560]{1,0:T(8,128)(2,1)}, u32[]{:S(2)}) copy-start(bf16[1024,2560]{1,0:T(8,128)(2,1)} %all-gather.2.cloned.1.call-done.refs_1_.w_up) | copy-start | bytes 15728644
  181.2 15.7 %copy-start.1 = (bf16[1024,2560]{1,0:T(8,128)(2,1)S(1)}, bf16[1024,2560]{1,0:T(8,128)(2,1)}, u32[]{:S(2)}) copy-start(bf16[1024,2560]{1,0:T(8,128)(2,1)} %all-gather.2.cloned.1.call-done.refs_1_.w_up) | copy-start | bytes 15728644
  196.9 8.8 %copy-start.6 = (bf16[2048,32]{0,1:T(8,128)(2,1)S(1)}, bf16[2048,32]{0,1:T(8,128)(2,1)}, u32[]{:S(2)}) copy-start(bf16[2048,32]{0,1:T(8,128)(2,1)} %param.23) | copy-start | bytes 393220
  206.6 10.6 %all-to-all-start.6 = ((f32[8,16,128]{2,1,0:T(8,128)}), f32[8,16,128]{2,1,0:T(8,128)S(1)}, u32[]{:S(2)}, u32[]{:S(2)}) async-start(f32[8,16,128]{2,1,0:T(8,128)} %shard_map.142), calls=%async_computation.6 | async-start | bytes 131072 | tf_op jit(solution)/shard_map/all_to_all | solution.py:23
Sparse Core Ops, SparseCore 0:
  10.1 148.0 all-gather.1
